TPU v7x, 32 devices: a whole 2x2x4 slice. The times are simulated.
32 devices in a mesh: sp: 16 (over z, y, x), tp: 2 (over core).
Axes of the slice: x: 2, y: 2, z: 4, core: 2. Of those that a mesh axis runs over, the one named last changes fastest.
Arguments:
- query_matrix: bfloat16 [4096, 2048], P('sp', 'tp'), may hold values from -6 to 6
- key_matrix: bfloat16 [4096, 2048], P('sp', 'tp'), may hold values from -6 to 6
- value_matrix: bfloat16 [4096, 2048], P('sp', 'tp'), may hold values from -6 to 6
- output_gate_logits: bfloat16 [4096, 2048], P('sp', 'tp'), may hold values from -6 to 6
- decay_preactivation: bfloat16 [4096, 2048], P('sp', 'tp'), may hold values from -3 to 12
- head_extra_decay: float32 [4096, 32], P('sp', 'tp'), may hold values from -0.7 to 0
- residual: bfloat16 [4096, 2048], P(('sp', 'tp')), may hold values from -6 to 6
- head_norm_gain: float32 [64], replicated, may hold values from 0.1 to 1.9
- output_projection_weight: bfloat16 [2048, 2048], P('tp'), may hold values from -0.125 to 0.125
- mixer_norm_gain: float32 [2048], replicated, may hold values from 0.1 to 1.9
- routes: int32 [4096, 2], P(('sp', 'tp')), may hold values from 0 to 15, all different within a row; in each aligned block of 128 rows (0 to 127, 128 to 255, ...) at most 32 rows name the same one
- routing_weight: float32 [4096, 2], P(('sp', 'tp')), may hold values from 0.2 to 1.5
- routed_gate_weight: bfloat16 [16, 2048, 1024], P('sp', None, 'tp'), may hold values from -0.125 to 0.125
- routed_up_weight: bfloat16 [16, 2048, 1024], P('sp', None, 'tp'), may hold values from -0.125 to 0.125
- routed_down_weight: bfloat16 [16, 1024, 2048], P('sp', 'tp'), may hold values from -0.1875 to 0.1875
- common_gate_weight: bfloat16 [2048, 512], replicated, may hold values from -0.125 to 0.125
- common_up_weight: bfloat16 [2048, 512], replicated, may hold values from -0.125 to 0.125
- common_down_weight: bfloat16 [512, 2048], replicated, may hold values from -0.25 to 0.25
- final_norm_gain: float32 [2048], replicated, may hold values from 0.1 to 1.9
Outputs:
- layer_out: bfloat16 [4096, 2048], P(('sp', 'tp'))
Inputs may be any that keep to these rules, and one draw needn't show every extreme that they name: `routes`: each row names 2 different experts. In the rows of one device (aligned blocks of rows) no expert is named by more than 32 rows, a bound that some block reaches.
All inputs are finite; a program needn't handle non-finite values.
Results may differ from a plain program's by a relative error of at most 0.019.
Values may be sent and summed in bfloat16 or wider, within the bound.
A program may use at most 192 MiB of HBM per device.

v0:
```python
import functools

import jax
import jax.numpy as jnp
from jax import lax
from jax.experimental import pallas as pl
from jax.experimental.pallas import tpu as pltpu
from jax.sharding import PartitionSpec as P

KEY_HEAD_SIZE = 64
BLOCK_TOKENS = 64


EPS = 1e-06
GATE_DIVISOR = 16.0


def layer_norm(values, gain):
    center = values - jnp.mean(values, axis=-1, keepdims=True)
    spread = jnp.mean(center * center, axis=-1, keepdims=True)
    return center * lax.rsqrt(spread + EPS) * gain


LANES = 128
MESH = pl.DeviceIdType.MESH


def lane_half(rows):
    return lax.broadcasted_iota(jnp.int32, (rows, LANES), 1) < KEY_HEAD_SIZE


def local_kernel(q_ref, k_ref, v_ref, decay_ref, extra_ref, out_ref, wide_ref, state_ref, total_ref):
    pair = pl.program_id(0)
    tokens = q_ref.shape[0]
    heads = extra_ref.shape[1]
    block = BLOCK_TOKENS
    half = lane_half(tokens)
    decay = decay_ref[...].astype(jnp.float32)
    logarithm = jnp.minimum(decay, 0.0) - jnp.log1p(jnp.exp(-jnp.abs(decay)))
    row = lax.broadcasted_iota(jnp.int32, (heads, LANES), 0)
    lane = lax.broadcasted_iota(jnp.int32, (heads, LANES), 1)
    chosen = (row == pair * (LANES // KEY_HEAD_SIZE) + lane // KEY_HEAD_SIZE).astype(jnp.float32)
    extra = jnp.dot(
        extra_ref[...], chosen, precision=lax.Precision.HIGHEST, preferred_element_type=jnp.float32
    )
    logarithm = logarithm * (1.0 / GATE_DIVISOR) + extra
    at = lax.broadcasted_iota(jnp.int32, (tokens, tokens), 0)
    other = lax.broadcasted_iota(jnp.int32, (tokens, tokens), 1)
    summed = jnp.dot(
        (other <= at).astype(jnp.float32),
        logarithm,
        precision=lax.Precision.HIGHEST,
        preferred_element_type=jnp.float32,
    )
    total = summed[tokens - 1 : tokens]
    query = q_ref[...].astype(jnp.float32) * KEY_HEAD_SIZE ** (-0.5)
    key = k_ref[...].astype(jnp.float32)
    value = v_ref[...]
    grown, rest = jnp.exp(summed), jnp.exp(total - summed)
    wide_ref[:, :LANES] = (query * grown).astype(jnp.bfloat16)
    wide_ref[:, LANES:] = (query * rest).astype(jnp.bfloat16)
    over = (((0,), (0,)), ((), ()))
    left = lax.dot_general(
        (key * rest).astype(jnp.bfloat16), value, over, preferred_element_type=jnp.float32
    )
    right = lax.dot_general(
        (key * grown).astype(jnp.bfloat16), value, over, preferred_element_type=jnp.float32
    )
    few = lane_half(KEY_HEAD_SIZE)
    top, low = slice(0, KEY_HEAD_SIZE), slice(KEY_HEAD_SIZE, LANES)
    first = jnp.where(few, left[top], pltpu.roll(right[top], KEY_HEAD_SIZE, 1))
    second = jnp.where(few, pltpu.roll(left[low], KEY_HEAD_SIZE, 1), right[low])
    state_ref[top] = first.astype(jnp.bfloat16)
    state_ref[low] = second.astype(jnp.bfloat16)
    total_ref[0] = total
    apart = (((1,), (1,)), ((), ()))
    small = lane_half(block)
    for place in range(tokens // block):
        begin, end = place * block, (place + 1) * block
        own = summed[begin:end]
        before = summed[begin - 1 : begin] if place else jnp.zeros((1, LANES), jnp.float32)
        after = summed[end - 1 : end]
        mine = query[begin:end]
        ups = mine * jnp.exp(own - before)
        tails = mine * jnp.exp(after - own)
        ups = jnp.concatenate([jnp.where(small, ups, 0.0), jnp.where(small, 0.0, ups)], axis=0)
        tails = jnp.concatenate(
            [jnp.where(small, tails, 0.0), jnp.where(small, 0.0, tails)], axis=0
        )
        key_left = key * jnp.exp(jnp.minimum(before - summed, 64.0))
        key_right = key * jnp.exp(jnp.minimum(summed - after, 64.0))
        ahead = lax.dot_general(
            ups.astype(jnp.bfloat16),
            key_left.astype(jnp.bfloat16),
            apart,
            preferred_element_type=jnp.float32,
        )
        behind = lax.dot_general(
            tails.astype(jnp.bfloat16),
            key_right.astype(jnp.bfloat16),
            apart,
            preferred_element_type=jnp.float32,
        )
        here = lax.broadcasted_iota(jnp.int32, (2 * block, tokens), 0)
        here = jnp.where(here < block, here, here - block) + begin
        there = lax.broadcasted_iota(jnp.int32, (2 * block, tokens), 1)
        scores = jnp.where(there <= here, ahead, behind).astype(jnp.bfloat16)
        both = jnp.dot(scores, value, preferred_element_type=jnp.float32)
        out_ref[begin:end] = jnp.where(small, both[:block], both[block:])


def local_part(query, key, value, decay, extra):
    tokens, width = query.shape
    pairs = width // LANES
    column = pl.BlockSpec((tokens, LANES), lambda p: (0, p))
    return pl.pallas_call(
        local_kernel,
        grid=(pairs,),
        in_specs=[column] * 4 + [pl.BlockSpec(extra.shape, lambda p: (0, 0))],
        out_specs=[
            column,
            pl.BlockSpec((tokens, 2 * LANES), lambda p: (0, p)),
            pl.BlockSpec((LANES, LANES), lambda p: (p, 0)),
            pl.BlockSpec((1, 1, LANES), lambda p: (p, 0, 0)),
        ],
        out_shape=[
            jax.ShapeDtypeStruct((tokens, width), jnp.float32),
            jax.ShapeDtypeStruct((tokens, 2 * width), jnp.bfloat16),
            jax.ShapeDtypeStruct((width, LANES), jnp.bfloat16),
            jax.ShapeDtypeStruct((pairs, 1, LANES), jnp.float32),
        ],
        name="local_part",
    )(query, key, value, decay, extra)


def exchange_kernel(
    n,
    state_ref,
    total_ref,
    out_ref,
    arrived,
    totals,
    ordered,
    before,
    outbound,
    send_state,
    recv_state,
    send_total,
    recv_total,
    send_back,
    recv_back,
):
    me = lax.axis_index("sp")
    rows = state_ref.shape[0] // n
    barrier = pltpu.get_barrier_semaphore()

    def greet(off, c):
        pl.semaphore_signal(
            barrier, inc=1, device_id={"sp": lax.rem(me + off, n)}, device_id_type=MESH
        )
        return c

    lax.fori_loop(1, n, greet, 0)
    pl.semaphore_wait(barrier, n - 1)

    def forth(off):
        to = lax.rem(me + off, n)
        first = pltpu.make_async_remote_copy(
            src_ref=state_ref.at[pl.ds(pl.multiple_of(to * rows, rows), rows)],
            dst_ref=arrived.at[off],
            send_sem=send_state.at[off],
            recv_sem=recv_state.at[off],
            device_id={"sp": to},
            device_id_type=MESH,
        )
        second = pltpu.make_async_remote_copy(
            src_ref=total_ref,
            dst_ref=totals.at[off],
            send_sem=send_total.at[off],
            recv_sem=recv_total.at[off],
            device_id={"sp": to},
            device_id_type=MESH,
        )
        return first, second

    def back(off):
        to = lax.rem(me + off, n)
        return pltpu.make_async_remote_copy(
            src_ref=outbound.at[to],
            dst_ref=out_ref.at[pl.ds(pl.multiple_of(me * rows, rows), rows)],
            send_sem=send_back.at[off],
            recv_sem=recv_back.at[off],
            device_id={"sp": to},
            device_id_type=MESH,
        )

    def start_forth(off, c):
        for copy in forth(off):
            copy.start()
        return c

    def wait_forth(off, c):
        for copy in forth(off):
            copy.wait()
        return c

    def start_back(off, c):
        back(off).start()
        return c

    def wait_back(off, c):
        back(off).wait()
        return c

    lax.fori_loop(1, n, start_forth, 0)
    mine = pl.ds(pl.multiple_of(me * rows, rows), rows)
    arrived[0] = state_ref[mine]
    totals[0] = total_ref[...]
    ordered[...] = jnp.zeros_like(ordered)
    lax.fori_loop(1, n, wait_forth, 0)
    group, shift = me * rows // LANES, lax.rem(me * rows, LANES)
    for k in range(n):
        ordered[k : k + 1] = totals[lax.rem(me - k + n, n), group]
    turned = pltpu.roll(ordered[...], lax.rem(LANES - shift, LANES), 1)
    weights = jnp.exp(turned.T)[:rows]
    half = lane_half(rows)
    carried = jnp.zeros((rows, LANES), jnp.float32)
    for k in range(n):
        before[k] = carried
        if k < n - 1:
            carried = weights[:, k : k + 1] * carried + arrived[lax.rem(me - k + n, n)].astype(
                jnp.float32
            )
    carried = jnp.zeros((rows, LANES), jnp.float32)
    for k in range(n - 1, -1, -1):
        outbound[k] = jnp.where(half, before[k], carried).astype(jnp.bfloat16)
        if k:
            carried = weights[:, k : k + 1] * carried + arrived[lax.rem(me - k + n, n)].astype(
                jnp.float32
            )
    lax.fori_loop(1, n, start_back, 0)
    out_ref[mine] = outbound[me]
    lax.fori_loop(1, n, wait_back, 0)


def exchange(state, total):
    n = lax.axis_size("sp")
    rows = state.shape[0] // n
    dma = pltpu.SemaphoreType.DMA((n,))
    return pl.pallas_call(
        functools.partial(exchange_kernel, n),
        in_specs=[pl.BlockSpec(memory_space=pltpu.VMEM)] * 2,
        out_specs=pl.BlockSpec(memory_space=pltpu.VMEM),
        out_shape=jax.ShapeDtypeStruct(state.shape, state.dtype),
        scratch_shapes=[
            pltpu.VMEM((n, rows, LANES), state.dtype),
            pltpu.VMEM((n,) + total.shape, jnp.float32),
            pltpu.VMEM((LANES, LANES), jnp.float32),
            pltpu.VMEM((n, rows, LANES), jnp.float32),
            pltpu.VMEM((n, rows, LANES), state.dtype),
            dma,
            dma,
            dma,
            dma,
            dma,
            dma,
        ],
        compiler_params=pltpu.CompilerParams(collective_id=0, has_side_effects=True),
        name="exchange",
    )(state, total)


def finish_kernel(local_ref, wide_ref, state_ref, logits_ref, gain_ref, out_ref):
    few = lane_half(KEY_HEAD_SIZE)
    first = state_ref[:KEY_HEAD_SIZE].astype(jnp.float32)
    second = state_ref[KEY_HEAD_SIZE:].astype(jnp.float32)
    states = jnp.concatenate(
        [
            jnp.where(few, first, 0.0),
            jnp.where(few, 0.0, pltpu.roll(second, KEY_HEAD_SIZE, 1)),
            jnp.where(few, pltpu.roll(first, KEY_HEAD_SIZE, 1), 0.0),
            jnp.where(few, 0.0, second),
        ],
        axis=0,
    ).astype(jnp.bfloat16)
    mixed = local_ref[...] + jnp.dot(wide_ref[...], states, preferred_element_type=jnp.float32)
    half = lane_half(mixed.shape[0])
    squares = mixed * mixed
    one = jnp.sum(jnp.where(half, squares, 0.0), axis=1, keepdims=True)
    two = jnp.sum(jnp.where(half, 0.0, squares), axis=1, keepdims=True)
    scale = jnp.where(
        half, lax.rsqrt(one / KEY_HEAD_SIZE + EPS), lax.rsqrt(two / KEY_HEAD_SIZE + EPS)
    )
    gate = jax.nn.silu(logits_ref[...].astype(jnp.float32))
    out_ref[...] = (mixed * scale * gain_ref[...] * gate).astype(jnp.bfloat16)


def finish_part(local, wide, state, logits, gain):
    tokens, width = local.shape
    column = pl.BlockSpec((tokens, LANES), lambda p: (0, p))
    return pl.pallas_call(
        finish_kernel,
        grid=(width // LANES,),
        in_specs=[
            column,
            pl.BlockSpec((tokens, 2 * LANES), lambda p: (0, p)),
            pl.BlockSpec((LANES, LANES), lambda p: (p, 0)),
            column,
            pl.BlockSpec((1, LANES), lambda p: (0, 0)),
        ],
        out_specs=column,
        out_shape=jax.ShapeDtypeStruct((tokens, width), jnp.bfloat16),
        name="finish_part",
    )(local, wide, state, logits, gain)


GROUP = 4


def expert_kernel(
    n,
    sent_ref,
    gate_hbm,
    up_hbm,
    down_hbm,
    result_ref,
    rows_in,
    gate_ref,
    up_ref,
    down_ref,
    kept,
    given,
    taken,
    summed,
    send_out,
    recv_out,
    send_row,
    recv_row,
    send_part,
    recv_part,
    send_back,
    recv_back,
    local,
):
    me, core = lax.axis_index("sp"), lax.axis_index("tp")
    groups = n // GROUP
    capacity, width = sent_ref.shape[1:]
    peer = {"tp": 1 - core}

    def target(off):
        high = lax.rem(me // GROUP + off // GROUP, groups)
        return high * GROUP + lax.rem(lax.rem(me, GROUP) + lax.rem(off, GROUP), GROUP)

    def origin(off):
        high = lax.rem(me // GROUP - off // GROUP + groups, groups)
        return high * GROUP + lax.rem(lax.rem(me, GROUP) - lax.rem(off, GROUP) + GROUP, GROUP)

    def remote(source, destination, send, recv, device):
        return pltpu.make_async_remote_copy(
            src_ref=source,
            dst_ref=destination,
            send_sem=send,
            recv_sem=recv,
            device_id=device,
            device_id_type=MESH,
        )

    def outward(off):
        return remote(
            sent_ref.at[target(off)],
            rows_in.at[off // GROUP, 0, lax.rem(off, GROUP)],
            send_out.at[off],
            recv_out.at[off],
            {"sp": target(off)},
        )

    def homeward(off):
        return remote(
            summed.at[off // GROUP, lax.rem(off, GROUP)],
            result_ref.at[me],
            send_back.at[off],
            recv_back.at[off],
            {"sp": origin(off)},
        )

    loads = [
        pltpu.make_async_copy(gate_hbm, gate_ref, local.at[0]),
        pltpu.make_async_copy(up_hbm, up_ref, local.at[1]),
        pltpu.make_async_copy(down_hbm, down_ref, local.at[2]),
        pltpu.make_async_copy(sent_ref.at[me], rows_in.at[0, 0, 0], local.at[3]),
    ]
    for load in loads:
        load.start()
    barrier = pltpu.get_barrier_semaphore()

    def greet(off, c):
        pl.semaphore_signal(barrier, inc=1, device_id={"sp": target(off)}, device_id_type=MESH)
        return c

    lax.fori_loop(1, n, greet, 0)
    pl.semaphore_signal(barrier, inc=1, device_id=peer, device_id_type=MESH)
    pl.semaphore_wait(barrier, n)

    def start_outward(off, c):
        outward(off).start()
        return c

    lax.fori_loop(1, n, start_outward, 0)
    for load in loads:
        load.wait()

    def arrive(off, c):
        outward(off).wait_recv()
        return c

    def start_homeward(off, c):
        homeward(off).start()
        return c

    def step(group, c):
        begin = group * GROUP
        skip = 1 - (group + groups - 1) // groups
        lax.fori_loop(begin + skip, begin + GROUP, arrive, 0)
        share = remote(
            rows_in.at[group, 0],
            rows_in.at[group, 1],
            send_row.at[group],
            recv_row.at[group],
            peer,
        )
        share.start()
        share.wait()
        rows = rows_in[group].reshape(2 * GROUP * capacity, width)
        gate = jnp.dot(rows, gate_ref[...], preferred_element_type=jnp.float32)
        up = jnp.dot(rows, up_ref[...], preferred_element_type=jnp.float32)
        inner = (jax.nn.silu(gate) * up).astype(jnp.bfloat16)
        part = jnp.dot(inner, down_ref[...], preferred_element_type=jnp.float32)
        part = part.astype(jnp.bfloat16).reshape(2, GROUP, capacity, width)
        given[group] = part[1]
        kept[...] = part[0]
        trade = remote(
            given.at[group], taken.at[group], send_part.at[group], recv_part.at[group], peer
        )
        trade.start()
        trade.wait()
        summed[group] = (
            kept[...].astype(jnp.float32) + taken[group].astype(jnp.float32)
        ).astype(jnp.bfloat16)
        lax.fori_loop(begin + skip, begin + GROUP, start_homeward, 0)
        return c

    lax.fori_loop(0, groups, step, 0)
    result_ref[me] = summed[0, 0]

    def finish(off, c):
        outward(off).wait_send()
        homeward(off).wait()
        return c

    lax.fori_loop(1, n, finish, 0)


def expert_exchange(sent, gate_half, up_half, down_half):
    n, capacity, width = sent.shape
    groups = n // GROUP
    block = (groups, GROUP, capacity, width)
    each, few = pltpu.SemaphoreType.DMA((n,)), pltpu.SemaphoreType.DMA((groups,))
    vmem, anywhere = pl.BlockSpec(memory_space=pltpu.VMEM), pl.BlockSpec(memory_space=pl.ANY)
    return pl.pallas_call(
        functools.partial(expert_kernel, n),
        in_specs=[vmem] + [anywhere] * 3,
        out_specs=vmem,
        out_shape=jax.ShapeDtypeStruct(sent.shape, sent.dtype),
        scratch_shapes=[
            pltpu.VMEM((groups, 2) + block[1:], sent.dtype),
            pltpu.VMEM(gate_half.shape, gate_half.dtype),
            pltpu.VMEM(up_half.shape, up_half.dtype),
            pltpu.VMEM(down_half.shape, down_half.dtype),
            pltpu.VMEM(block[1:], sent.dtype),
            pltpu.VMEM(block, sent.dtype),
            pltpu.VMEM(block, sent.dtype),
            pltpu.VMEM(block, sent.dtype),
            each,
            each,
            few,
            few,
            few,
            few,
            each,
            each,
            pltpu.SemaphoreType.DMA((4,)),
        ],
        compiler_params=pltpu.CompilerParams(collective_id=1, has_side_effects=True),
        name="expert_exchange",
    )(sent, gate_half, up_half, down_half)


def per_device(
    query_matrix,
    key_matrix,
    value_matrix,
    output_gate_logits,
    decay_preactivation,
    head_extra_decay,
    residual,
    head_norm_gain,
    output_projection_weight,
    mixer_norm_gain,
    routes,
    routing_weight,
    routed_gate_weight,
    routed_up_weight,
    routed_down_weight,
    common_gate_weight,
    common_up_weight,
    common_down_weight,
    final_norm_gain,
):
    local_out, wide, state, total = local_part(
        query_matrix, key_matrix, value_matrix, decay_preactivation, head_extra_decay
    )
    entered = exchange(state, total)
    gain = jnp.concatenate([head_norm_gain] * (LANES // KEY_HEAD_SIZE))[None]
    gated = finish_part(local_out, wide, entered, output_gate_logits, gain)
    projected = lax.psum_scatter(
        jnp.dot(gated, output_projection_weight, preferred_element_type=jnp.float32).astype(
            jnp.bfloat16
        ),
        "tp",
        scatter_dimension=0,
        tiled=True,
    ).astype(jnp.float32)
    normed = layer_norm(residual.astype(jnp.float32) + projected, mixer_norm_gain).astype(
        jnp.bfloat16
    )
    row_count = normed.shape[0]
    model_width = normed.shape[1]
    top_count = routes.shape[1]
    experts = lax.axis_size("sp")
    capacity = max(2, row_count * top_count // experts * 2)
    flat_expert = routes.reshape(-1)
    member = (flat_expert[:, None] == jnp.arange(experts, dtype=jnp.int32)[None, :]).astype(
        jnp.int32
    )
    rank_in = jnp.sum((jnp.cumsum(member, axis=0) - member) * member, axis=1)
    slot_of = flat_expert * capacity + rank_in
    source_row = (
        jnp.zeros((experts * capacity,), jnp.int32)
        .at[slot_of]
        .set(jnp.arange(row_count * top_count, dtype=jnp.int32) // top_count)
    )
    outbound = normed[source_row].reshape(experts, capacity, model_width)
    gate_half = routed_gate_weight[0]
    up_half = routed_up_weight[0]
    down_half = routed_down_weight[0]
    expert_out = expert_exchange(outbound, gate_half, up_half, down_half)
    flat_out = expert_out.reshape(experts * capacity, model_width)
    picked = flat_out[slot_of].astype(jnp.float32).reshape(row_count, top_count, model_width)
    routed = jnp.einsum("rk,rkd->rd", routing_weight, picked)
    shared_gate_out = jnp.dot(normed, common_gate_weight, preferred_element_type=jnp.float32)
    shared_up_out = jnp.dot(normed, common_up_weight, preferred_element_type=jnp.float32)
    shared_inner = (jax.nn.silu(shared_gate_out) * shared_up_out).astype(jnp.bfloat16)
    feed = jnp.dot(shared_inner, common_down_weight, preferred_element_type=jnp.float32) + routed
    return layer_norm(normed.astype(jnp.float32) + feed, final_norm_gain).astype(jnp.bfloat16)


def solution(mesh):
    placed = (
        P("sp", "tp"),
        P("sp", "tp"),
        P("sp", "tp"),
        P("sp", "tp"),
        P("sp", "tp"),
        P("sp", "tp"),
        P(("sp", "tp"), None),
        P(),
        P("tp", None),
        P(),
        P(("sp", "tp"), None),
        P(("sp", "tp"), None),
        P("sp", None, "tp"),
        P("sp", None, "tp"),
        P("sp", "tp", None),
        P(),
        P(),
        P(),
        P(),
    )
    return jax.shard_map(
        per_device, mesh=mesh, in_specs=placed, out_specs=P(("sp", "tp"), None), check_vma=False
    )
```

profile of v0, /device:TPU:0, one launch (start us, length us, event | category | flops | bytes accessed | tf_op | source)
XLA Modules:
  0.0 216.8 jit_solution(4023506712270147756)
XLA Ops:
  6.5 0.0 copy-start
  6.5 0.0 reduce-scatter.2.cloned.1.call-start
  6.5 1.6 copy.21.extra_ref
  8.2 1.3 maximum_bitcast_fusion.gain_ref
  9.5 16.4 %local_part.1 = (f32[256,1024]{1,0:T(8,128)}, bf16[256,2048]{1,0:T(8,128)(2,1)}, bf16[1024,128]{1,0:T(8,128)(2,1)}, f32[8,1,128]{2,1,0:T(1,128)}) custom-call(bf16[256,1024]{1,0:T(8,128)(2,1)} %q_ref.1, bf16[256,1024]{1,0:T(8,128)(2,1)} %k_ref.1, bf16[256,1024]{1,0:T(8,128)(2,1)} %v_ref.1, bf16[256,1024]{1,0:T(8,128)(2,1)} %decay_ref.1, ...), custom_call_target="tpu_custom_call" | custom-call | tf_op jit(solution)/shard_map/local_part/pallas_call | solution.py:116
  25.9 24.1 %exchange.1.state_ref = bf16[1024,128]{1,0:T(8,128)(2,1)} custom-call(bf16[1024,128]{1,0:T(8,128)(2,1)} %get-tuple-element.11.state_ref, f32[8,1,128]{2,1,0:T(1,128)} %get-tuple-element.12.total_ref), custom_call_target="tpu_custom_call" | custom-call | tf_op jit(solution)/shard_map/exchange/pallas_call | solution.py:250
  50.0 6.9 %finish_part.1 = bf16[256,1024]{1,0:T(8,128)(2,1)} custom-call(f32[256,1024]{1,0:T(8,128)} %get-tuple-element.9.local_ref, bf16[256,2048]{1,0:T(8,128)(2,1)} %get-tuple-element.10.wide_ref, bf16[1024,128]{1,0:T(8,128)(2,1)} %exchange.1.state_ref, bf16[256,1024]{1,0:T(8,128)(2,1)} %logits_ref.1, f32[1,128]{1,0:T(1,128)} %maximum_bitcast_fusion.gain_ref), custom_call_target="tpu_custom_call" | custom-call | tf_op jit(solution)/shard_map/finish_part/pallas_call | solution.py:301
  56.9 0.0 copy-start.6
  56.9 0.0 copy-start.7
  56.9 0.0 copy-start.1
  56.9 4.6 %convolution_convert_fusion = bf16[256,2048]{1,0:T(8,128)(2,1)} fusion(bf16[256,1024]{1,0:T(8,128)(2,1)} %finish_part.1, bf16[1024,2048]{1,0:T(8,128)(2,1)} %param.27), kind=kOutput, calls=%fused_computation.3 | convolution fusion | flops 1074266112 | bytes 5767168 | tf_op jit(solution)/shard_map/dot_general | solution.py:526
  61.5 0.0 copy-start.4
  61.5 0.0 reduce-scatter.2.cloned.1.call-update
  61.6 0.0 copy-done.6
  61.6 0.1 copy.23
  61.7 0.1 eq.29
  61.8 0.1 eq.25
  62.0 0.6 reduce-window.6
  62.6 0.2 slice_reduce_fusion
  62.8 0.1 copy.22
  62.9 0.1 mul.73
  63.1 0.0 copy-done.7
  63.1 0.2 copy.26
  63.2 0.1 fusion.12
  63.3 1.6 scatter_custom_fusion
  65.0 6.0 %reduce-scatter.2.cloned.1.call-done = bf16[128,2048]{1,0:T(8,128)(2,1)} async-done(((bf16[256,2048]{1,0:T(8,128)(2,1)}), bf16[128,2048]{1,0:T(8,128)(2,1)}) %reduce-scatter.2.cloned.1.call-update) | async-done | bytes 524304 | tf_op jit(solution)/shard_map/reduce_scatter | solution.py:525
  70.9 0.0 copy-done.1
  70.9 0.0 copy-start.2
  70.9 1.3 fusion.3
  72.3 1.3 multiply_reduce_fusion.1
  73.6 0.0 copy-done.4
  73.6 0.0 copy-done.2
  73.6 0.3 multiply_convert_fusion.1
  73.9 3.3 %gather_fusion = bf16[512,2048]{1,0:T(8,128)(2,1)} fusion(bf16[128,2048]{1,0:T(8,128)(2,1)S(1)} %multiply_convert_fusion.1, s32[1024]{0:T(1024)S(1)} %pad_clamp_fusion.1), kind=kCustom, calls=%fused_computation | custom fusion | bytes 4196352 | tf_op jit(solution)/shard_map/gather | solution.py:552
  77.2 112.9 %expert_exchange.1 = bf16[16,32,2048]{2,1,0:T(8,128)(2,1)} custom-call(bf16[16,32,2048]{2,1,0:T(8,128)(2,1)} %bitcast.41, bf16[2048,512]{1,0:T(8,128)(2,1)} %bitcast.42, bf16[2048,512]{1,0:T(8,128)(2,1)} %bitcast.43, bf16[512,2048]{1,0:T(8,128)(2,1)} %bitcast.44), custom_call_target="tpu_custom_call" | custom-call | tf_op jit(solution)/shard_map/expert_exchange/pallas_call | solution.py:469
  190.1 5.2 %gather_fusion.1 = bf16[256,2048]{1,0:T(8,128)(2,1)} fusion(bf16[512,2048]{1,0:T(8,128)(2,1)} %bitcast.40, s32[1024]{0:T(1024)S(1)} %pad_clamp_fusion), kind=kCustom, calls=%fused_computation.1 | custom fusion | bytes 2098176 | tf_op jit(solution)/shard_map/gather | solution.py:558
  195.3 2.5 %reshape.84 = bf16[128,2,2048]{2,1,0:T(2,128)(2,1)} reshape(bf16[256,2048]{1,0:T(8,128)(2,1)} %gather_fusion.1) | data formatting | bytes 2097152 | tf_op jit(solution)/shard_map/reshape | solution.py:558
  197.9 0.0 copy-start.3
  197.9 2.1 fusion.18
  200.0 0.0 copy-done.3
  200.0 2.2 %fusion.19 = f32[128,1,2048]{2,1,0:T(1,128)} fusion(bf16[128,2,2048]{2,1,0:T(2,128)(2,1)S(1)} %copy-done.3, bf16[128,2,1]{1,2,0:T(2,128)(2,1)S(1)} %copy.26), kind=kOutput, calls=%fused_computation.49 | convolution fusion | flops 1048576 | bytes 2097664 | tf_op jit(solution)/shard_map/rk,rkd->rd/dot_general | solution.py:559
  202.2 0.0 copy-done
  202.2 0.0 copy-start.5
  202.2 4.0 %fusion.17 = (f32[128]{0:T(128)S(1)}, f32[128,2048]{1,0:T(8,128)}) fusion(f32[128,1,2048]{2,1,0:T(1,128)} %fusion.19, bf16[512,2048]{1,0:T(8,128)(2,1)S(1)} %copy-done, bf16[128,2048]{1,0:T(8,128)(2,1)S(1)} %multiply_convert_fusion.1, bf16[2048,512]{1,0:T(8,128)(2,1)} %param.35, f32[128,512]{1,0:T(8,128)S(1)} %fusion.18), kind=kOutput, calls=%fused_computation.47 | convolution fusion | flops 538312576 | bytes 7078400 | tf_op jit(solution)/shard_map/dot_general | solution.py:563
  206.2 1.5 multiply_reduce_fusion
  207.7 0.0 copy-done.5
  207.7 2.2 %multiply_convert_fusion = bf16[128,2048]{1,0:T(8,128)(2,1)} fusion(f32[128,2048]{1,0:T(8,128)} %get-tuple-element.14, f32[2048]{0:T(1024)S(1)} %copy-done.5, f32[128]{0:T(128)S(1)} %add_rsqrt_fusion, f32[128]{0:T(128)S(1)} %broadcast_multiply_fusion.1), kind=kLoop, calls=%fused_computation.8 | loop fusion | flops 1048576 | bytes 1582080 | tf_op jit(solution)/shard_map/convert_element_type | solution.py:564
  (13 shorter events, 0.1 us)
Async XLA Ops:
  6.5 195.7 %copy-start = (bf16[512,2048]{1,0:T(8,128)(2,1)S(1)}, bf16[512,2048]{1,0:T(8,128)(2,1)}, u32[]{:S(2)}) copy-start(bf16[512,2048]{1,0:T(8,128)(2,1)} %param.36) | copy-start | bytes 6291460
  6.5 64.4 %reduce-scatter.2.cloned.1.call-start = ((), (), s32[]{:S(2)}) async-start(), calls=%async_computation.1 | async-start | bytes 1572864 | tf_op jit(solution)/shard_map/reduce_scatter | solution.py:525
  56.9 4.7 %copy-start.6 = (s32[128,2]{0,1:T(2,128)S(1)}, s32[128,2]{0,1:T(2,128)}, u32[]{:S(2)}) copy-start(s32[128,2]{0,1:T(2,128)} %param.29) | copy-start | bytes 3076
  56.9 6.2 %copy-start.7 = (f32[128,2]{0,1:T(2,128)S(1)}, f32[128,2]{0,1:T(2,128)}, u32[]{:S(2)}) copy-start(f32[128,2]{0,1:T(2,128)} %param.30) | copy-start | bytes 3076
  56.9 14.1 %copy-start.1 = (bf16[128,2048]{1,0:T(8,128)(2,1)S(1)}, bf16[128,2048]{1,0:T(8,128)(2,1)}, u32[]{:S(2)}) copy-start(bf16[128,2048]{1,0:T(8,128)(2,1)} %param.25) | copy-start | bytes 1572868
  61.5 12.1 %copy-start.4 = (f32[2048]{0:T(1024)S(1)}, f32[2048]{0:T(1024)}, u32[]{:S(2)}) copy-start(f32[2048]{0:T(1024)} %param.28) | copy-start | bytes 24580
  70.9 2.7 %copy-start.2 = (bf16[128,2048]{1,0:T(8,128)(2,1)S(1)}, bf16[128,2048]{1,0:T(8,128)(2,1)}, u32[]{:S(2)}) copy-start(bf16[128,2048]{1,0:T(8,128)(2,1)} %reduce-scatter.2.cloned.1.call-done) | copy-start | bytes 1572868
  197.9 2.1 copy-start.3
  202.2 5.5 %copy-start.5 = (f32[2048]{0:T(1024)S(1)}, f32[2048]{0:T(1024)}, u32[]{:S(2)}) copy-start(f32[2048]{0:T(1024)} %param.37) | copy-start | bytes 24580
Sparse Core Ops, SparseCore 0:
  61.7 9.1 reduce-scatter.1
where the time goes:
time: 217 us
  Pallas kernels  160 us (74%)
  local copies, waits for them, and re-layouts  15.3 us (7%)
  between operations  13.6 us (6%)
  matrix products  13 us (6%)
  other arithmetic  8.74 us (4%)
  waiting for transfers between devices  5.97 us (3%)
    pallas_call x1, Pallas kernels, expert_exchange(): pl.pallas_call(functools.partial(expert_kernel, n), in_specs=[vmem] + [an...  113 us
    pallas_call x1, Pallas kernels, exchange(): pl.pallas_call(functools.partial(exchange_kernel, n), in_specs=[pl.BlockS...  24.1 us
    pallas_call x1, Pallas kernels, local_part(): pl.pallas_call(local_kernel, grid=(pairs,), in_specs=[column] * 4 + [pl.B...  16.4 us
    pallas_call x1, Pallas kernels, finish_part(): pl.pallas_call(finish_kernel, grid=(width // LANES,), in_specs=[column, p...  6.89 us
    reduce_scatter x1, waiting for transfers between devices, per_device(): lax.psum_scatter(jnp.dot(gated, output_projection_weight, preferred_eleme...  5.96 us
    gather x1, local copies, waits for them, and re-layouts, per_device(): flat_out[slot_of].astype(jnp.float32)  5.21 us
    dot_general x1, matrix products, per_device(): jnp.dot(gated, output_projection_weight, preferred_element_type=jnp.float32)  4.65 us
  transfers between devices with their start and end apart: 1, of which 1 were waited for; matrix products, arithmetic and copies ran while one was open for 2% of the time, Pallas kernels for 0%

commit v1 on v0

v1 whole, which is shorter than its diff:
```python
import functools

import jax
import jax.numpy as jnp
from jax import lax
from jax.experimental import pallas as pl
from jax.experimental.pallas import tpu as pltpu
from jax.sharding import PartitionSpec as P

KEY_HEAD_SIZE = 64
BLOCK_TOKENS = 64
EPS = 1e-06
GATE_DIVISOR = 16.0
LANES = 128
PLANES = 4
CHUNKS = 2
COLUMNS = 512
NORM_ROWS = 16
MESH = pl.DeviceIdType.MESH
OVER = (((0,), (0,)), ((), ()))
APART = (((1,), (1,)), ((), ()))


def lane_half(rows):
    return lax.broadcasted_iota(jnp.int32, (rows, LANES), 1) < KEY_HEAD_SIZE


def layer_norm(values, gain):
    center = values - jnp.mean(values, axis=-1, keepdims=True)
    spread = jnp.mean(center * center, axis=-1, keepdims=True)
    return center * lax.rsqrt(spread + EPS) * gain


def three(values):
    high = values.astype(jnp.bfloat16)
    rest = values - high.astype(jnp.float32)
    middle = rest.astype(jnp.bfloat16)
    low = (rest - middle.astype(jnp.float32)).astype(jnp.bfloat16)
    return high, middle, low


def product(left, right, dims=(((1,), (0,)), ((), ()))):
    return lax.dot_general(left, right, dims, preferred_element_type=jnp.float32)


def remote(source, destination, send, recv, device):
    return pltpu.make_async_remote_copy(
        src_ref=source,
        dst_ref=destination,
        send_sem=send,
        recv_sem=recv,
        device_id=device,
        device_id_type=MESH,
    )


def repeat(begin, end, body):
    def step(i, c):
        body(i)
        return c

    lax.fori_loop(begin, end, step, 0)


def columns_of(i, width=COLUMNS):
    return pl.ds(pl.multiple_of(i * width, width), width)


def mixer_kernel(
    n,
    q_ref,
    k_ref,
    v_ref,
    logits_ref,
    decay_ref,
    extra_ref,
    residual_ref,
    gain_ref,
    norm_gain_ref,
    weight_hbm,
    out_ref,
    weight_ref,
    summed_ref,
    wide_ref,
    local_ref,
    state_ref,
    total_ref,
    arrived,
    totals,
    ordered,
    before_ref,
    outbound,
    entered,
    gated_ref,
    given,
    taken,
    kept,
    send_state,
    recv_state,
    send_total,
    recv_total,
    send_back,
    recv_back,
    load_sem,
    send_part,
    recv_part,
):
    me, core = lax.axis_index("sp"), lax.axis_index("tp")
    peer = {"tp": 1 - core}
    tokens, width = q_ref.shape
    heads = extra_ref.shape[0]
    pairs = width // LANES
    rows = width // n
    owners = LANES // rows
    block = BLOCK_TOKENS
    model = weight_ref.shape[1]
    load = pltpu.make_async_copy(weight_hbm, weight_ref, load_sem)
    load.start()
    barrier = pltpu.get_barrier_semaphore()

    def greet(off):
        pl.semaphore_signal(
            barrier, inc=1, device_id={"sp": lax.rem(me + off, n)}, device_id_type=MESH
        )

    repeat(1, n, greet)
    pl.semaphore_signal(barrier, inc=1, device_id=peer, device_id_type=MESH)

    def forth(to):
        first = remote(
            state_ref.at[pl.ds(pl.multiple_of(to * rows, rows), rows)],
            arrived.at[me],
            send_state.at[to],
            recv_state.at[me],
            {"sp": to},
        )
        second = remote(
            total_ref.at[to // owners],
            totals.at[me],
            send_total.at[to],
            recv_total.at[me],
            {"sp": to},
        )
        return first, second

    def forth_in(source):
        first = remote(
            state_ref.at[pl.ds(0, rows)],
            arrived.at[source],
            send_state.at[source],
            recv_state.at[source],
            {"sp": source},
        )
        second = remote(
            total_ref.at[0],
            totals.at[source],
            send_total.at[source],
            recv_total.at[source],
            {"sp": source},
        )
        return first, second

    def back(to):
        return remote(
            outbound.at[to],
            entered.at[pl.ds(pl.multiple_of(me * rows, rows), rows)],
            send_back.at[to],
            recv_back.at[me],
            {"sp": to},
        )

    def back_in(source):
        return remote(
            outbound.at[source],
            entered.at[pl.ds(pl.multiple_of(source * rows, rows), rows)],
            send_back.at[source],
            recv_back.at[source],
            {"sp": source},
        )

    triangle = (
        lax.broadcasted_iota(jnp.int32, (tokens, tokens), 1)
        <= lax.broadcasted_iota(jnp.int32, (tokens, tokens), 0)
    ).astype(jnp.bfloat16)
    few = lane_half(KEY_HEAD_SIZE)
    half = lane_half(tokens)
    top, low = slice(0, KEY_HEAD_SIZE), slice(KEY_HEAD_SIZE, LANES)

    def prepare(step):
        pair = lax.rem(step + me // owners, pairs)
        lanes = columns_of(pair, LANES)
        decay = decay_ref[:, lanes].astype(jnp.float32)
        logarithm = jnp.minimum(decay, 0.0) - jnp.log1p(jnp.exp(-jnp.abs(decay)))
        row = lax.broadcasted_iota(jnp.int32, (heads, LANES), 0)
        lane = lax.broadcasted_iota(jnp.int32, (heads, LANES), 1)
        chosen = (row == pair * (LANES // KEY_HEAD_SIZE) + lane // KEY_HEAD_SIZE).astype(
            jnp.bfloat16
        )
        extra = sum(product(piece, chosen, OVER) for piece in three(extra_ref[...]))
        logarithm = logarithm * (1.0 / GATE_DIVISOR) + extra
        summed = sum(product(triangle, piece) for piece in three(logarithm))
        total = summed[tokens - 1 : tokens]
        summed_ref[pair] = summed
        query = q_ref[:, lanes].astype(jnp.float32) * KEY_HEAD_SIZE ** (-0.5)
        key = k_ref[:, lanes].astype(jnp.float32)
        value = v_ref[:, lanes]
        grown, rest = jnp.exp(summed), jnp.exp(total - summed)
        wide_ref[pair, :, :LANES] = (query * grown).astype(jnp.bfloat16)
        wide_ref[pair, :, LANES:] = (query * rest).astype(jnp.bfloat16)
        left = product((key * rest).astype(jnp.bfloat16), value, OVER)
        right = product((key * grown).astype(jnp.bfloat16), value, OVER)
        first = jnp.where(few, left[top], pltpu.roll(right[top], KEY_HEAD_SIZE, 1))
        second = jnp.where(few, pltpu.roll(left[low], KEY_HEAD_SIZE, 1), right[low])
        begin = pl.multiple_of(pair * LANES, LANES)
        state_ref[pl.ds(begin, LANES)] = jnp.concatenate([first, second], axis=0).astype(
            jnp.bfloat16
        )
        total_ref[pair] = total

        @pl.when(step == 0)
        def _():
            pl.semaphore_wait(barrier, n)

        def start(j):
            to = pair * owners + j

            @pl.when(to != me)
            def _():
                for copy in forth(to):
                    copy.start()

        repeat(0, owners, start)

    def attend(pair):
        lanes = columns_of(pair, LANES)
        summed = summed_ref[pair]
        query = q_ref[:, lanes].astype(jnp.float32) * KEY_HEAD_SIZE ** (-0.5)
        key = k_ref[:, lanes].astype(jnp.float32)
        value = v_ref[:, lanes]
        small = lane_half(block)
        for place in range(tokens // block):
            begin, end = place * block, (place + 1) * block
            own = summed[begin:end]
            before = summed[begin - 1 : begin] if place else jnp.zeros((1, LANES), jnp.float32)
            after = summed[end - 1 : end]
            mine = query[begin:end]
            ups = mine * jnp.exp(own - before)
            tails = mine * jnp.exp(after - own)
            ups = jnp.concatenate([jnp.where(small, ups, 0.0), jnp.where(small, 0.0, ups)], axis=0)
            tails = jnp.concatenate(
                [jnp.where(small, tails, 0.0), jnp.where(small, 0.0, tails)], axis=0
            )
            key_left = key[:end] * jnp.exp(jnp.minimum(before - summed[:end], 64.0))
            key_right = key[begin:] * jnp.exp(jnp.minimum(summed[begin:] - after, 64.0))
            ahead = product(ups.astype(jnp.bfloat16), key_left.astype(jnp.bfloat16), APART)
            behind = product(tails.astype(jnp.bfloat16), key_right.astype(jnp.bfloat16), APART)

            def place_of(size):
                here = lax.broadcasted_iota(jnp.int32, (2 * block, size), 0)
                return jnp.where(here < block, here, here - block)

            there = lax.broadcasted_iota(jnp.int32, (2 * block, end), 1)
            ahead = jnp.where(there <= place_of(end) + begin, ahead, 0.0)
            there = lax.broadcasted_iota(jnp.int32, (2 * block, tokens - begin), 1)
            behind = jnp.where(there > place_of(tokens - begin), behind, 0.0)
            both = product(ahead.astype(jnp.bfloat16), value[:end]) + product(
                behind.astype(jnp.bfloat16), value[begin:]
            )
            local_ref[pair, begin:end] = jnp.where(small, both[:block], both[block:])

    def finish(pair):
        lanes = columns_of(pair, LANES)
        begin = pl.multiple_of(pair * LANES, LANES)
        state = entered[pl.ds(begin, LANES)].astype(jnp.float32)
        first, second = state[top], state[low]
        states = jnp.concatenate(
            [
                jnp.where(few, first, 0.0),
                jnp.where(few, 0.0, pltpu.roll(second, KEY_HEAD_SIZE, 1)),
                jnp.where(few, pltpu.roll(first, KEY_HEAD_SIZE, 1), 0.0),
                jnp.where(few, 0.0, second),
            ],
            axis=0,
        ).astype(jnp.bfloat16)
        mixed = local_ref[pair] + product(wide_ref[pair], states)
        squares = mixed * mixed
        one = jnp.sum(jnp.where(half, squares, 0.0), axis=1, keepdims=True)
        two = jnp.sum(jnp.where(half, 0.0, squares), axis=1, keepdims=True)
        scale = jnp.where(
            half, lax.rsqrt(one / KEY_HEAD_SIZE + EPS), lax.rsqrt(two / KEY_HEAD_SIZE + EPS)
        )
        gate = jax.nn.silu(logits_ref[:, lanes].astype(jnp.float32))
        gated_ref[:, lanes] = (mixed * scale * gain_ref[...] * gate).astype(jnp.bfloat16)

    repeat(0, pairs, prepare)
    repeat(0, pairs // 2, attend)
    mine = pl.ds(pl.multiple_of(me * rows, rows), rows)
    arrived[me] = state_ref[mine]
    totals[me] = total_ref[me // owners]

    def wait_forth(off):
        for copy in forth_in(lax.rem(me + off, n)):
            copy.wait_recv()

    repeat(1, n, wait_forth)
    ordered[...] = jnp.zeros_like(ordered)
    for k in range(n):
        ordered[k : k + 1] = totals[k]
    turned = pltpu.roll(ordered[...], lax.rem(LANES - lax.rem(me * rows, LANES), LANES), 1)
    weights = jnp.exp(turned.T)[:rows]
    carried = jnp.zeros((rows, LANES), jnp.float32)
    for k in range(n):
        before_ref[k] = carried
        if k < n - 1:
            carried = weights[:, k : k + 1] * carried + arrived[k].astype(jnp.float32)
    carried = jnp.zeros((rows, LANES), jnp.float32)
    first_half = lane_half(rows)
    for k in range(n - 1, -1, -1):
        outbound[k] = jnp.where(first_half, before_ref[k], carried).astype(jnp.bfloat16)
        if k:
            carried = weights[:, k : k + 1] * carried + arrived[k].astype(jnp.float32)

    repeat(1, n, lambda off: back(lax.rem(me + off, n)).start())
    entered[mine] = outbound[me]
    repeat(pairs // 2, pairs, attend)
    repeat(1, n, lambda off: back_in(lax.rem(me + off, n)).wait_recv())
    repeat(0, pairs, finish)
    load.wait()
    few_rows = tokens // 2
    theirs = pl.ds(pl.multiple_of((1 - core) * few_rows, few_rows), few_rows)
    ours = pl.ds(pl.multiple_of(core * few_rows, few_rows), few_rows)

    def trade(i):
        return remote(
            given.at[:, columns_of(i)],
            taken.at[:, columns_of(i)],
            send_part.at[i],
            recv_part.at[i],
            peer,
        )

    def project_theirs(i):
        given[:, columns_of(i)] = product(
            gated_ref[theirs, :], weight_ref[:, columns_of(i)]
        ).astype(jnp.bfloat16)
        trade(i).start()

    def project_ours(i):
        kept[:, columns_of(i)] = product(
            gated_ref[ours, :], weight_ref[:, columns_of(i)]
        ).astype(jnp.bfloat16)

    parts = model // COLUMNS
    repeat(0, parts, project_theirs)
    repeat(0, parts, project_ours)
    repeat(0, parts, lambda i: trade(i).wait_recv())

    def normalize(i):
        some = pl.ds(pl.multiple_of(i * NORM_ROWS, NORM_ROWS), NORM_ROWS)
        projected = kept[some].astype(jnp.float32) + taken[some].astype(jnp.float32)
        out_ref[some] = layer_norm(
            residual_ref[some].astype(jnp.float32) + projected, norm_gain_ref[...]
        ).astype(jnp.bfloat16)

    repeat(0, few_rows // NORM_ROWS, normalize)

    def sent(off):
        to = lax.rem(me + off, n)
        for copy in forth(to):
            copy.wait_send()
        back(to).wait_send()

    repeat(1, n, sent)
    repeat(0, parts, lambda i: trade(i).wait_send())


def mixer(query, key, value, logits, decay, extra, residual, gain, norm_gain, weight):
    n = lax.axis_size("sp")
    tokens, width = query.shape
    pairs, rows, model = width // LANES, width // n, weight.shape[1]
    half = (tokens // 2, model)
    vmem, anywhere = pl.BlockSpec(memory_space=pltpu.VMEM), pl.BlockSpec(memory_space=pl.ANY)
    each = pltpu.SemaphoreType.DMA((n,))
    parts = pltpu.SemaphoreType.DMA((model // COLUMNS,))
    return pl.pallas_call(
        functools.partial(mixer_kernel, n),
        in_specs=[vmem] * 9 + [anywhere],
        out_specs=vmem,
        out_shape=jax.ShapeDtypeStruct(half, jnp.bfloat16),
        scratch_shapes=[
            pltpu.VMEM(weight.shape, jnp.bfloat16),
            pltpu.VMEM((pairs, tokens, LANES), jnp.float32),
            pltpu.VMEM((pairs, tokens, 2 * LANES), jnp.bfloat16),
            pltpu.VMEM((pairs, tokens, LANES), jnp.float32),
            pltpu.VMEM((width, LANES), jnp.bfloat16),
            pltpu.VMEM((pairs, 1, LANES), jnp.float32),
            pltpu.VMEM((n, rows, LANES), jnp.bfloat16),
            pltpu.VMEM((n, 1, LANES), jnp.float32),
            pltpu.VMEM((LANES, LANES), jnp.float32),
            pltpu.VMEM((n, rows, LANES), jnp.float32),
            pltpu.VMEM((n, rows, LANES), jnp.bfloat16),
            pltpu.VMEM((width, LANES), jnp.bfloat16),
            pltpu.VMEM((tokens, width), jnp.bfloat16),
            pltpu.VMEM(half, jnp.bfloat16),
            pltpu.VMEM(half, jnp.bfloat16),
            pltpu.VMEM(half, jnp.bfloat16),
            each,
            each,
            each,
            each,
            each,
            each,
            pltpu.SemaphoreType.DMA(()),
            parts,
            parts,
        ],
        compiler_params=pltpu.CompilerParams(collective_id=0, has_side_effects=True),
        name="mixer",
    )(query, key, value, logits, decay, extra, residual, gain, norm_gain, weight)


def expert_kernel(
    n,
    normed_ref,
    routes_ref,
    routing_ref,
    gain_ref,
    gate_hbm,
    up_hbm,
    down_hbm,
    common_gate_hbm,
    common_up_hbm,
    common_down_hbm,
    out_ref,
    gate_ref,
    up_ref,
    down_ref,
    common_gate,
    common_up,
    common_down,
    meta,
    gathered,
    picked,
    rows_in,
    given,
    taken,
    kept,
    summed,
    returned,
    feed,
    load_sem,
    send_meta,
    recv_meta,
    send_line,
    recv_line,
    send_pick,
    recv_pick,
    copy_pick,
    send_share,
    recv_share,
    send_part,
    recv_part,
    send_back,
    recv_back,
):
    me, core = lax.axis_index("sp"), lax.axis_index("tp")
    peer = {"tp": 1 - core}
    members = n // PLANES
    plane, member = me // members, lax.rem(me, members)
    rows, width = normed_ref.shape
    capacity = returned.shape[1]
    slots = members * capacity
    inner = (plane > 0) & (plane < PLANES - 1)
    parts = width // COLUMNS
    chunk = rows // CHUNKS

    def source_at(k):
        low = plane < PLANES // 2
        one = jnp.where(low, plane + 1, plane - 1)
        two = jnp.where(low, 2 - 2 * plane, 7 - 2 * plane)
        three_ = jnp.where(low, PLANES - 1, 0)
        return jnp.where(k == 0, plane, jnp.where(k == 1, one, jnp.where(k == 2, two, three_)))

    loads = [
        pltpu.make_async_copy(common_gate_hbm, common_gate, load_sem.at[0]),
        pltpu.make_async_copy(common_up_hbm, common_up, load_sem.at[1]),
        pltpu.make_async_copy(common_down_hbm, common_down, load_sem.at[2]),
        pltpu.make_async_copy(gate_hbm, gate_ref, load_sem.at[3]),
        pltpu.make_async_copy(up_hbm, up_ref, load_sem.at[4]),
        pltpu.make_async_copy(down_hbm, down_ref, load_sem.at[5]),
    ]
    own = pltpu.make_async_copy(normed_ref, gathered.at[plane], load_sem.at[6])
    own.start()
    barrier = pltpu.get_barrier_semaphore()

    def greet(device):
        pl.semaphore_signal(barrier, inc=1, device_id=device, device_id_type=MESH)

    for off in range(1, PLANES):
        greet({"sp": lax.rem(plane + off, PLANES) * members + member})
    repeat(1, members, lambda q: greet({"sp": plane * members + lax.rem(member + q, members)}))
    greet(peer)
    for load in loads:
        load.start()
    expert = lax.broadcasted_iota(jnp.int32, (n, rows), 0)
    one = (expert == routes_ref[0:1]).astype(jnp.float32)
    two = (expert == routes_ref[1:2]).astype(jnp.float32)
    earlier = (
        lax.broadcasted_iota(jnp.int32, (rows, rows), 0)
        < lax.broadcasted_iota(jnp.int32, (rows, rows), 1)
    ).astype(jnp.bfloat16)
    rank = product((one + two).astype(jnp.bfloat16), earlier)
    place = (expert * capacity).astype(jnp.float32) + rank
    meta[plane] = jnp.zeros(meta.shape[1:], jnp.float32)
    meta[plane, 0:1] = jnp.sum(one * place, axis=0, keepdims=True)
    meta[plane, 1:2] = jnp.sum(two * place, axis=0, keepdims=True)
    meta[plane, 2:4] = routing_ref[...]

    def tell(to):
        return remote(
            meta.at[plane],
            meta.at[plane],
            send_meta.at[to],
            recv_meta.at[plane],
            {"sp": to * members + member},
        )

    def told(source):
        return remote(
            meta.at[source],
            meta.at[source],
            send_meta.at[source],
            recv_meta.at[source],
            {"sp": source * members + member},
        )

    def part_of(c):
        return pl.ds(pl.multiple_of(c * chunk, chunk), chunk)

    def along(source, c, up):
        piece = gathered.at[source, part_of(c)]
        return remote(
            piece,
            piece,
            send_line.at[2 * source + up, c],
            recv_line.at[source, c],
            {"sp": me + (2 * up - 1) * members},
        )

    def along_own(c, up):
        return remote(
            normed_ref.at[part_of(c)],
            gathered.at[plane, part_of(c)],
            send_line.at[2 * plane + up, c],
            recv_line.at[plane, c],
            {"sp": me + (2 * up - 1) * members},
        )

    def arrive(source, c):
        along(source, c, 0).wait_recv()

        @pl.when(inner & (source < plane))
        def _():
            along(source, c, 1).start()

        @pl.when(inner & (source > plane))
        def _():
            along(source, c, 0).start()

    def outward(source, to):
        return remote(
            picked.at[source, to],
            rows_in.at[source, 0, member],
            send_pick.at[source, to],
            recv_pick.at[source, member],
            {"sp": plane * members + to},
        )

    def inward(source, origin):
        return remote(
            picked.at[source, origin],
            rows_in.at[source, 0, origin],
            send_pick.at[source, origin],
            recv_pick.at[source, origin],
            {"sp": plane * members + origin},
        )

    def stay(source):
        return pltpu.make_async_copy(
            picked.at[source, member], rows_in.at[source, 0, member], copy_pick.at[source]
        )

    def sharing(source):
        return remote(
            rows_in.at[source, 0],
            rows_in.at[source, 1],
            send_share.at[source],
            recv_share.at[source],
            peer,
        )

    def trading(source):
        return remote(
            given.at[source], taken.at[source], send_part.at[source], recv_part.at[source], peer
        )

    def homeward(source, to):
        target = source * members + to
        return remote(
            summed.at[source, to],
            returned.at[me],
            send_back.at[target],
            recv_back.at[me],
            {"sp": target},
        )

    def homecoming(origin):
        return remote(
            summed.at[0, 0],
            returned.at[origin],
            send_back.at[origin],
            recv_back.at[origin],
            {"sp": origin},
        )

    def dispatch(source):
        slot = lax.broadcasted_iota(jnp.int32, (slots, rows), 0) + plane * slots
        slot = slot.astype(jnp.float32)
        table = meta[source]
        wanted = ((slot == table[0:1]) | (slot == table[1:2])).astype(jnp.bfloat16)

        def some(i):
            values = product(wanted, gathered[source, :, columns_of(i)]).astype(jnp.bfloat16)
            picked[source, :, :, columns_of(i)] = values.reshape(members, capacity, COLUMNS)

        repeat(0, parts, some)
        repeat(1, members, lambda q: outward(source, lax.rem(member + q, members)).start())
        stay(source).start()

    def share(source):
        repeat(1, members, lambda q: inward(source, lax.rem(member + q, members)).wait_recv())
        stay(source).wait()
        sharing(source).start()

    def compute(source):
        sharing(source).wait_recv()
        values = rows_in[source].reshape(2 * slots, width)
        gate = product(values, gate_ref[...])
        up = product(values, up_ref[...])
        hidden = (jax.nn.silu(gate) * up).astype(jnp.bfloat16)
        part = product(hidden, down_ref[...]).astype(jnp.bfloat16)
        part = part.reshape(2, members, capacity, width)
        given[source] = part[1]
        kept[source] = part[0]
        trading(source).start()

    def home(source):
        trading(source).wait_recv()
        summed[source] = (
            kept[source].astype(jnp.float32) + taken[source].astype(jnp.float32)
        ).astype(jnp.bfloat16)

        def start(q):
            to = lax.rem(member + q, members)

            @pl.when((source != plane) | (q > 0))
            def _():
                homeward(source, to).start()

        repeat(0, members, start)

    pl.semaphore_wait(barrier, PLANES - 1 + members)
    for off in range(1, PLANES):
        tell(lax.rem(plane + off, PLANES)).start()
    for c in range(CHUNKS):

        @pl.when(plane < PLANES - 1)
        def _():
            along_own(c, 1).start()

        @pl.when(plane > 0)
        def _():
            along_own(c, 0).start()

    own.wait()
    dispatch(plane)
    for load in loads[:3]:
        load.wait()
    gate = product(normed_ref[...], common_gate[...])
    up = product(normed_ref[...], common_up[...])
    hidden = (jax.nn.silu(gate) * up).astype(jnp.bfloat16)

    def shared(i):
        feed[:, columns_of(i)] = normed_ref[:, columns_of(i)].astype(jnp.float32) + product(
            hidden, common_down[:, columns_of(i)]
        )

    repeat(0, parts, shared)
    for off in range(1, PLANES):
        told(lax.rem(plane + off, PLANES)).wait_recv()

    @pl.when(inner)
    def _():
        arrive(source_at(1), 0)
        arrive(source_at(2), 0)

    share(plane)
    for load in loads[3:]:
        load.wait()

    def step(k):
        source, following = source_at(k), source_at(k + 1)
        more = k < PLANES - 1

        @pl.when(inner & (k == 0))
        def _():
            arrive(source_at(1), 1)
            arrive(source_at(2), 1)

        @pl.when(inner & (k > 0) & more)
        def _():
            arrive(source_at(3), k - 1)

        @pl.when(jnp.logical_not(inner) & more)
        def _():
            for c in range(CHUNKS):
                arrive(following, c)

        @pl.when(more)
        def _():
            dispatch(following)

        compute(source)
        home(source)

        @pl.when(more)
        def _():
            share(following)

    repeat(0, PLANES, step)
    returned[me] = summed[plane, member]

    def combine(k):
        source = source_at(k)

        def come(q):
            origin = source * members + lax.rem(member + q, members)

            @pl.when(origin != me)
            def _():
                homecoming(origin).wait_recv()

        repeat(0, members, come)
        slot = lax.broadcasted_iota(jnp.int32, (slots, rows), 0) + source * slots
        slot = slot.astype(jnp.float32)
        table = meta[plane]
        share_of = jnp.where(slot == table[0:1], table[2:3], 0.0)
        share_of = share_of + jnp.where(slot == table[1:2], table[3:4], 0.0)
        high = share_of.astype(jnp.bfloat16)
        low = (share_of - high.astype(jnp.float32)).astype(jnp.bfloat16)
        begin = pl.multiple_of(source * members, members)

        def some(i):
            values = returned[pl.ds(begin, members), :, columns_of(i)].reshape(slots, COLUMNS)
            feed[:, columns_of(i)] += product(high, values, OVER) + product(low, values, OVER)

        repeat(0, parts, some)

    repeat(0, PLANES, combine)

    def normalize(i):
        some = pl.ds(pl.multiple_of(i * NORM_ROWS, NORM_ROWS), NORM_ROWS)
        out_ref[some] = layer_norm(feed[some], gain_ref[...]).astype(jnp.bfloat16)

    repeat(0, rows // NORM_ROWS, normalize)

    for off in range(1, PLANES):
        tell(lax.rem(plane + off, PLANES)).wait_send()
    for c in range(CHUNKS):

        @pl.when(plane < PLANES - 1)
        def _():
            along_own(c, 1).wait_send()

        @pl.when(plane > 0)
        def _():
            along_own(c, 0).wait_send()

        for source in range(PLANES):

            @pl.when(inner & (source < plane))
            def _():
                along(source, c, 1).wait_send()

            @pl.when(inner & (source > plane))
            def _():
                along(source, c, 0).wait_send()

    def sent(source):
        repeat(1, members, lambda q: outward(source, lax.rem(member + q, members)).wait_send())
        sharing(source).wait_send()
        trading(source).wait_send()

        def gone(q):
            to = lax.rem(member + q, members)

            @pl.when((source != plane) | (q > 0))
            def _():
                homeward(source, to).wait_send()

        repeat(0, members, gone)

    repeat(0, PLANES, sent)


def experts(normed, routes, routing, gain, capacity, weights):
    n = lax.axis_size("sp")
    rows, width = normed.shape
    members = n // PLANES
    kind = normed.dtype
    group = (PLANES, members, capacity, width)
    vmem, anywhere = pl.BlockSpec(memory_space=pltpu.VMEM), pl.BlockSpec(memory_space=pl.ANY)

    def dma(*shape):
        return pltpu.SemaphoreType.DMA(shape)

    return pl.pallas_call(
        functools.partial(expert_kernel, n),
        in_specs=[vmem] * 4 + [anywhere] * 6,
        out_specs=vmem,
        out_shape=jax.ShapeDtypeStruct(normed.shape, kind),
        scratch_shapes=[pltpu.VMEM(w.shape, w.dtype) for w in weights]
        + [
            pltpu.VMEM((PLANES, 8, rows), jnp.float32),
            pltpu.VMEM((PLANES, rows, width), kind),
            pltpu.VMEM(group, kind),
            pltpu.VMEM((PLANES, 2) + group[1:], kind),
            pltpu.VMEM(group, kind),
            pltpu.VMEM(group, kind),
            pltpu.VMEM(group, kind),
            pltpu.VMEM(group, kind),
            pltpu.VMEM((n, capacity, width), kind),
            pltpu.VMEM((rows, width), jnp.float32),
            dma(7),
            dma(PLANES),
            dma(PLANES),
            dma(2 * PLANES, CHUNKS),
            dma(PLANES, CHUNKS),
            dma(PLANES, members),
            dma(PLANES, members),
            dma(PLANES),
            dma(PLANES),
            dma(PLANES),
            dma(PLANES),
            dma(PLANES),
            dma(n),
            dma(n),
        ],
        compiler_params=pltpu.CompilerParams(collective_id=1, has_side_effects=True),
        name="experts",
    )(normed, routes, routing, gain, *weights)


def per_device(
    query_matrix,
    key_matrix,
    value_matrix,
    output_gate_logits,
    decay_preactivation,
    head_extra_decay,
    residual,
    head_norm_gain,
    output_projection_weight,
    mixer_norm_gain,
    routes,
    routing_weight,
    routed_gate_weight,
    routed_up_weight,
    routed_down_weight,
    common_gate_weight,
    common_up_weight,
    common_down_weight,
    final_norm_gain,
):
    gain = jnp.concatenate([head_norm_gain] * (LANES // KEY_HEAD_SIZE))[None]
    normed = mixer(
        query_matrix,
        key_matrix,
        value_matrix,
        output_gate_logits,
        decay_preactivation,
        head_extra_decay.T,
        residual,
        gain,
        mixer_norm_gain[None],
        output_projection_weight,
    )
    row_count, top_count = routes.shape
    capacity = max(2, row_count * top_count // lax.axis_size("sp") * 2)
    return experts(
        normed,
        routes.T,
        routing_weight.T,
        final_norm_gain[None],
        capacity,
        (
            routed_gate_weight[0],
            routed_up_weight[0],
            routed_down_weight[0],
            common_gate_weight,
            common_up_weight,
            common_down_weight,
        ),
    )


def solution(mesh):
    placed = (
        P("sp", "tp"),
        P("sp", "tp"),
        P("sp", "tp"),
        P("sp", "tp"),
        P("sp", "tp"),
        P("sp", "tp"),
        P(("sp", "tp"), None),
        P(),
        P("tp", None),
        P(),
        P(("sp", "tp"), None),
        P(("sp", "tp"), None),
        P("sp", None, "tp"),
        P("sp", None, "tp"),
        P("sp", "tp", None),
        P(),
        P(),
        P(),
        P(),
    )
    return jax.shard_map(
        per_device, mesh=mesh, in_specs=placed, out_specs=P(("sp", "tp"), None), check_vma=False
    )
```

time: 217 us -> 140 us (0.65)
  Pallas kernels: 160 us -> 135 us
  between operations: 13.6 us -> 0.02 us
  local copies, waits for them, and re-layouts: 15.3 us -> 1.88 us
  matrix products: 13 us -> 0 us
  other arithmetic: 8.74 us -> 1.31 us
  waiting for transfers between devices: 5.97 us -> 0 us
    pallas_call x4 -> x2, Pallas kernels: 160 us -> 135 us  [the longest x1 101 us: experts(): pl.pallas_call(functools.partial(expert_kernel, n), in_specs=[vmem] * 4 +...]
    dot_general x4 -> x0, matrix products: 13 us -> none  [the longest x1 4.65 us: per_device(): jnp.dot(gated, output_projection_weight, preferred_element_type=jnp.float32)]
    gather x2 -> x0, local copies, waits for them, and re-layouts: 8.5 us -> none  [the longest x1 5.21 us: per_device(): flat_out[slot_of].astype(jnp.float32)]
    reduce_scatter x1 -> x0, waiting for transfers between devices: 5.96 us -> none  [per_device(): lax.psum_scatter(jnp.dot(gated, output_projection_weight, preferred_eleme...]
    reduce_sum x4 -> x0, other arithmetic: 4.24 us -> none  [the longest x2 2.82 us: layer_norm(): spread = jnp.mean(center * center, axis=-1, keepdims=True)]
    reshape x1 -> x0, local copies, waits for them, and re-layouts: 2.54 us -> none  [per_device(): flat_out[slot_of].astype(jnp.float32)]
    convert_element_type x3 -> x0, other arithmetic: 2.5 us -> none  [the longest x1 2.22 us: per_device(): layer_norm(normed.astype(jnp.float32) + feed, final_norm_gain)]
  transfers between devices with their start and end apart: 1 -> 0, of which waited for: 1 -> 0; matrix products, arithmetic and copies ran while one was open for 2% -> 0% of each run, Pallas kernels for 0% -> 0%
where the time goes in v1:
time: 140 us; the launch traced here: 138 us
  Pallas kernels  135 us (96%)
  local copies, waits for them, and re-layouts  1.88 us (1%)
    pallas_call x1, Pallas kernels, experts(): pl.pallas_call(functools.partial(expert_kernel, n), in_specs=[vmem] * 4 +...  101 us
    pallas_call x1, Pallas kernels, mixer(): pl.pallas_call(functools.partial(mixer_kernel, n), in_specs=[vmem] * 9 +...  34.3 us

profile of v1, /device:TPU:0, one launch (start us, length us, event | category | flops | bytes accessed | tf_op | source)
XLA Modules:
  0.0 138.0 jit_solution(16837871091674537684)
XLA Ops:
  0.0 1.3 maximum_bitcast_fusion.gain_ref
  1.3 34.3 %mixer.1.normed_ref = bf16[128,2048]{1,0:T(8,128)(2,1)} custom-call(bf16[256,1024]{1,0:T(8,128)(2,1)} %q_ref.1, bf16[256,1024]{1,0:T(8,128)(2,1)} %k_ref.1, bf16[256,1024]{1,0:T(8,128)(2,1)} %v_ref.1, bf16[256,1024]{1,0:T(8,128)(2,1)} %logits_ref.1, bf16[256,1024]{1,0:T(8,128)(2,1)} %decay_ref.1, f32[16,256]{1,0:T(8,128)} %bitcast.13, ...), custom_call_target="tpu_custom_call" | custom-call | tf_op jit(solution)/shard_map/mixer/pallas_call | solution.py:385
  35.6 100.5 %experts.1 = bf16[128,2048]{1,0:T(8,128)(2,1)} custom-call(bf16[128,2048]{1,0:T(8,128)(2,1)} %mixer.1.normed_ref, s32[2,128]{1,0:T(2,128)} %bitcast.16, f32[2,128]{1,0:T(2,128)} %bitcast.17, f32[1,2048]{1,0:T(1,128)} %bitcast.15, bf16[2048,512]{1,0:T(8,128)(2,1)} %bitcast.10, bf16[2048,512]{1,0:T(8,128)(2,1)} %bitcast.11, bf16[512,2048]{1,0:T(8,128)(2,1)} %bitcast.12, ...), custom_call_target="tpu_custom_call" | custom-call | tf_op jit(solution)/shard_map/experts/pallas_call | solution.py:827
  136.1 1.9 %copy.21 = bf16[128,2048]{1,0:T(8,128)(2,1)} copy(bf16[128,2048]{1,0:T(8,128)(2,1)} %experts.1) | data formatting | bytes 1048576
